TPU v7x, 512 devices: a 8x2x16 block of a 8x8x16 slice. The times are simulated.
512 devices in a mesh: grp: 2 (over y), ep: 32 (over z, core), tp: 8 (over x).
Axes of the slice: x: 8, y: 2, z: 16, core: 2. Of those that a mesh axis runs over, the one named last changes fastest.
The devices are a block of a 8x8x16 slice.
Arguments:
- tokens: bfloat16 [16384, 2048], P(('grp', 'ep')), parts along dimension 0, may hold values from -6 to 6
- in_gain: bfloat16 [2048], replicated, may hold values from 0.099609375 to 1.8984375
- expert_ids: int32 [16384, 2], P(('grp', 'ep')), parts along dimension 0, may hold values from 0 to 31, all different within a row; in each aligned block of 256 rows (0 to 255, 256 to 511, ...) at most 32 rows name the same one
- route_weights: float32 [16384, 2], P(('grp', 'ep')), parts along dimension 0, may hold values from 0.1 to 1
- gate_weight: bfloat16 [32, 2048, 2048], P('ep', None, 'tp'), may hold values from -0.375 to 0.375
- up_weight: bfloat16 [32, 2048, 2048], P('ep', None, 'tp'), may hold values from -0.375 to 0.375
- down_weight: bfloat16 [32, 2048, 2048], P('ep', 'tp')
- out_gain: bfloat16 [2048], P('tp'), may hold values from 0.099609375 to 1.8984375
Outputs:
- normed_out: bfloat16 [16384, 2048], P(('grp', 'ep'), 'tp'), parts along dimension 0
There are 2 independent parts, one for each index of `grp`. A program takes and returns all parts, laid end to end along the dimension named above; an argument that names none is the same for every part. Nothing has to cross between parts.
Inputs may be any that keep to these rules, and one draw needn't show every extreme that they name: `expert_ids`: each row names 2 different experts. Among the 256 rows of one index of ep, no expert is named more than 32 times, a bound that some block reaches.
All inputs are finite; a program needn't handle non-finite values.
Results may differ from a plain program's by a relative error of at most 0.015.
Values may be sent and summed in bfloat16 or wider, within the bound.
A program may use at most 64 MiB of HBM per device.

v0:
```python
import jax
import jax.numpy as jnp
from jax import lax
from jax.sharding import PartitionSpec as P

eps = 1e-05


def copy_for_each(shard, axis):
    copies = jnp.broadcast_to(shard, (lax.axis_size(axis), *shard.shape))
    return lax.all_to_all(copies, axis, split_axis=0, concat_axis=0, tiled=True)


def of_everyone(shard, axis):
    everything = copy_for_each(shard, axis)
    return jnp.sum(everything, axis=0)


def on_device(
    tokens, in_gain, expert_ids, route_weights, gate_weight, up_weight, down_weight, out_gain
):
    n_ep = lax.axis_size("ep")
    n_tp = lax.axis_size("tp")
    tok_count, width = tokens.shape
    top_count = expert_ids.shape[1]
    experts = n_ep * gate_weight.shape[0]
    capacity = 2 * tok_count * top_count // experts
    feat_block = width // n_tp
    xf = tokens.astype(jnp.float32)
    normed_in = (
        xf * lax.rsqrt(jnp.mean(xf * xf, axis=1, keepdims=True) + eps) * in_gain.astype(jnp.float32)
    ).astype(jnp.bfloat16)
    flat_ids = expert_ids.reshape(-1)
    onehot = (flat_ids[:, None] == jnp.arange(experts, dtype=jnp.int32)[None, :]).astype(jnp.int32)
    slot = jnp.sum((jnp.cumsum(onehot, axis=0) - onehot) * onehot, axis=1)
    dest = flat_ids * capacity + slot
    token_of = jnp.arange(tok_count * top_count, dtype=jnp.int32) // top_count
    slot_token = jnp.full((experts * capacity,), tok_count, jnp.int32).at[dest].set(token_of)
    source = lax.dynamic_slice_in_dim(normed_in, lax.axis_index("tp") * feat_block, feat_block, 1)
    extended = jnp.concatenate([source, jnp.zeros((1, source.shape[1]), jnp.bfloat16)], axis=0)
    outgoing = extended[slot_token].reshape(experts, capacity, source.shape[1])
    w_gate = gate_weight[0]
    w_up = up_weight[0]
    arrived = lax.all_to_all(outgoing, "ep", split_axis=0, concat_axis=0, tiled=True).reshape(
        n_ep * capacity, feat_block
    )
    piece = lax.all_gather(arrived, "tp", axis=1, tiled=True)
    gate_pre = jnp.dot(piece, w_gate, preferred_element_type=jnp.float32)
    up_pre = jnp.dot(piece, w_up, preferred_element_type=jnp.float32)
    clamped = jnp.minimum(gate_pre, 7.0)
    bounded = jnp.clip(up_pre, -7.0, 7.0)
    act = (clamped * jax.nn.sigmoid(1.702 * clamped) * (bounded + 1.0)).astype(jnp.bfloat16)
    w_down = down_weight[0]
    summed = lax.psum_scatter(
        lax.dot_general(
            w_down, act, (((0,), (1,)), ((), ())), preferred_element_type=jnp.float32
        ).astype(jnp.bfloat16),
        "tp",
        scatter_dimension=0,
        tiled=True,
    )
    summed = summed.reshape(feat_block, n_ep, capacity)
    returned = lax.all_to_all(summed, "ep", split_axis=1, concat_axis=1, tiled=True)
    returned = returned.reshape(feat_block, experts * capacity).T
    picked = returned[dest].astype(jnp.float32).reshape(tok_count, top_count, feat_block)
    combined = jnp.sum(picked * route_weights[:, :, None], axis=1)
    squares = of_everyone(jnp.sum(combined * combined, axis=1), "tp")
    scale = lax.rsqrt(squares / width + eps)
    return (combined * scale[:, None] * out_gain.astype(jnp.float32)).astype(jnp.bfloat16)


def solution(mesh):
    placed = (
        P(("grp", "ep"), None),
        P(),
        P(("grp", "ep"), None),
        P(("grp", "ep"), None),
        P("ep", None, "tp"),
        P("ep", None, "tp"),
        P("ep", "tp", None),
        P("tp"),
    )
    return jax.shard_map(
        on_device, mesh=mesh, in_specs=placed, out_specs=P(("grp", "ep"), "tp"), check_vma=False
    )
```

profile of v0, /device:TPU:80, one launch (start us, length us, event | category | flops | bytes accessed | tf_op | source)
XLA Modules:
  0.0 301.2 jit_solution(15357068313004622765)
XLA Ops:
  6.5 0.0 copy-start
  6.6 0.0 copy-start.1
  6.6 0.0 all-gather.2.cloned.1.call-start
  6.6 1.6 convert_element_type.38
  8.1 1.5 multiply_reduce_fusion
  9.6 0.0 copy-done.1
  9.6 0.1 copy.21
  9.8 0.1 eq.29
  9.9 0.1 eq.25
  10.1 1.2 reduce-window.6
  11.3 0.2 slice_reduce_fusion
  11.6 0.1 copy.20
  11.7 0.1 mul.88
  11.9 0.1 fusion.21
  12.0 2.4 scatter_custom_fusion
  14.4 0.8 dynamic-slice
  15.2 0.1 fusion.18
  15.3 0.0 copy-start.3
  15.3 3.9 %gather_fusion = bf16[1024,256]{1,0:T(8,128)(2,1)S(1)} fusion(bf16[257,256]{1,0:T(8,128)(2,1)S(1)} %concatenate.3, s32[1024]{0:T(1024)S(1)} %fusion.23), kind=kCustom, calls=%fused_computation | custom fusion | bytes 1052672 | tf_op jit(solution)/shard_map/gather | solution.py:41
  19.3 77.5 %all_to_all.16 = bf16[32,32,256]{2,1,0:T(8,128)(2,1)} all-to-all(bf16[32,32,256]{2,1,0:T(8,128)(2,1)S(1)} %bitcast.43), channel_id=1, replica_groups=mesh['grp'=2,'ep'=32,'tp'=8] {'ep'}, dimensions={0} | all-to-all | bytes 1048576 | tf_op jit(solution)/shard_map/all_to_all | solution.py:44
  96.7 0.0 copy-start.4
  96.7 0.1 all-gather.2.cloned.1.call-update
  96.8 0.1 reduce-scatter.2.cloned.1.call-start
  96.9 60.0 %all-gather.2.cloned.1.call-done = bf16[1024,2048]{1,0:T(8,128)(2,1)} async-done(((bf16[1024,256]{1,0:T(8,128)(2,1)}), bf16[1024,2048]{1,0:T(8,128)(2,1)}) %all-gather.2.cloned.1.call-update) | async-done | bytes 4194320 | tf_op jit(solution)/shard_map/all_gather | solution.py:47
  156.9 0.0 copy-done.3
  156.9 4.5 %convolution_minimum_fusion = f32[1024,256]{1,0:T(8,128)} fusion(bf16[1024,2048]{1,0:T(8,128)(2,1)} %all-gather.2.cloned.1.call-done, bf16[1,2048,256]{2,1,0:T(8,128)(2,1)S(1)} %copy-done.3), kind=kOutput, calls=%fused_computation.5 | convolution fusion | flops 1074003968 | bytes 6291456 | tf_op jit(solution)/shard_map/dot_general | solution.py:48
  161.4 0.0 copy-done
  161.4 0.0 copy-done.4
  161.4 8.9 %convert_bitcast_fusion = bf16[2048,1024]{0,1:T(8,128)(2,1)} fusion(bf16[1024,2048]{1,0:T(8,128)(2,1)} %all-gather.2.cloned.1.call-done, bf16[1,256,2048]{2,1,0:T(8,128)(2,1)S(1)} %copy-done, bf16[1,2048,256]{2,1,0:T(8,128)(2,1)S(1)} %copy-done.4, f32[1024,256]{1,0:T(8,128)} %convolution_minimum_fusion), kind=kOutput, calls=%fused_computation.3 | convolution fusion | flops 2151940096 | bytes 11534336 | tf_op jit(solution)/shard_map/dot_general | solution.py:55
  170.3 0.0 copy-start.2
  170.3 0.0 copy-start.5
  170.3 0.1 reduce-scatter.2.cloned.1.call-update
  170.3 60.4 %reduce-scatter.2.cloned.1.call-done = bf16[256,1024]{0,1:T(8,128)(2,1)} async-done(((bf16[2048,1024]{0,1:T(8,128)(2,1)}), bf16[256,1024]{0,1:T(8,128)(2,1)}) %reduce-scatter.2.cloned.1.call-update) | async-done | bytes 524304 | tf_op jit(solution)/shard_map/reduce_scatter | solution.py:54
  230.7 13.8 %all-to-all-start.1 = ((bf16[256,32,32]{0,2,1:T(8,128)(2,1)}), bf16[256,32,32]{0,2,1:T(8,128)(2,1)S(1)}, u32[]{:S(2)}, u32[]{:S(2)}) async-start(bf16[256,32,32]{0,2,1:T(8,128)(2,1)} %bitcast.44), calls=%async_computation.2 | async-start | bytes 1048576 | tf_op jit(solution)/shard_map/all_to_all | solution.py:63
  244.5 0.0 copy-done.2
  244.5 0.1 copy.24
  244.7 32.9 %all-to-all-done.1 = bf16[256,32,32]{0,2,1:T(8,128)(2,1)S(1)} async-done(((bf16[256,32,32]{0,2,1:T(8,128)(2,1)}), bf16[256,32,32]{0,2,1:T(8,128)(2,1)S(1)}, u32[]{:S(2)}, u32[]{:S(2)}) %all-to-all-start.1) | async-done | bytes 524320 | tf_op jit(solution)/shard_map/all_to_all | solution.py:63
  277.6 1.9 gather_fusion.1
  279.6 0.3 reshape.87
  279.9 0.7 multiply_reduce_fusion.1
  280.6 0.1 multiply_reduce_fusion.2
  280.7 0.6 broadcast_in_dim.8
  281.3 4.5 %all-to-all-start.2 = ((f32[8,1,256]{2,1,0:T(1,128)}), f32[8,1,256]{2,1,0:T(1,128)S(1)}, u32[]{:S(2)}, u32[]{:S(2)}) async-start(f32[8,1,256]{2,1,0:T(1,128)} %broadcast_in_dim.8), calls=%async_computation.3 | async-start | bytes 16384 | tf_op jit(solution)/shard_map/all_to_all | solution.py:11
  285.8 0.0 copy-done.5
  285.8 7.7 %all-to-all-done.2 = f32[8,1,256]{2,1,0:T(1,128)S(1)} async-done(((f32[8,1,256]{2,1,0:T(1,128)}), f32[8,1,256]{2,1,0:T(1,128)S(1)}, u32[]{:S(2)}, u32[]{:S(2)}) %all-to-all-start.2) | async-done | bytes 8224 | tf_op jit(solution)/shard_map/all_to_all | solution.py:11
  293.6 0.8 multiply_convert_fusion
  (13 shorter events, 0.1 us)
Async XLA Ops:
  6.5 154.9 %copy-start = (bf16[1,256,2048]{2,1,0:T(8,128)(2,1)S(1)}, bf16[1,256,2048]{2,1,0:T(8,128)(2,1)}, u32[]{:S(2)}) copy-start(bf16[1,256,2048]{2,1,0:T(8,128)(2,1)} %param.14) | copy-start | bytes 3145732
  6.6 3.1 %copy-start.1 = (s32[256,2]{0,1:T(2,128)S(1)}, s32[256,2]{0,1:T(2,128)}, u32[]{:S(2)}) copy-start(s32[256,2]{0,1:T(2,128)} %param.10) | copy-start | bytes 6148
  6.6 150.3 %all-gather.2.cloned.1.call-start = ((), (), s32[]{:S(2)}) async-start(), calls=%async_computation.4 | async-start | bytes 4718592 | tf_op jit(solution)/shard_map/all_gather | solution.py:47
  15.3 141.6 %copy-start.3 = (bf16[1,2048,256]{2,1,0:T(8,128)(2,1)S(1)}, bf16[1,2048,256]{2,1,0:T(8,128)(2,1)}, u32[]{:S(2)}) copy-start(bf16[1,2048,256]{2,1,0:T(8,128)(2,1)} %param.12) | copy-start | bytes 3145732
  96.7 64.7 %copy-start.4 = (bf16[1,2048,256]{2,1,0:T(8,128)(2,1)S(1)}, bf16[1,2048,256]{2,1,0:T(8,128)(2,1)}, u32[]{:S(2)}) copy-start(bf16[1,2048,256]{2,1,0:T(8,128)(2,1)} %param.13) | copy-start | bytes 3145732
  96.8 133.9 %reduce-scatter.2.cloned.1.call-start = ((), (), s32[]{:S(2)}) async-start(), calls=%async_computation.5 | async-start | bytes 4718592 | tf_op jit(solution)/shard_map/reduce_scatter | solution.py:54
  170.3 74.3 %copy-start.2 = (f32[256,2]{0,1:T(2,128)S(1)}, f32[256,2]{0,1:T(2,128)}, u32[]{:S(2)}) copy-start(f32[256,2]{0,1:T(2,128)} %param.11) | copy-start | bytes 6148
  170.3 115.6 %copy-start.5 = (bf16[256]{0:T(256)(128)(2,1)S(1)}, bf16[256]{0:T(256)(128)(2,1)}, u32[]{:S(2)}) copy-start(bf16[256]{0:T(256)(128)(2,1)} %param.15) | copy-start | bytes 1540
  230.7 46.9 %all-to-all-start.1 = ((bf16[256,32,32]{0,2,1:T(8,128)(2,1)}), bf16[256,32,32]{0,2,1:T(8,128)(2,1)S(1)}, u32[]{:S(2)}, u32[]{:S(2)}) async-start(bf16[256,32,32]{0,2,1:T(8,128)(2,1)} %bitcast.44), calls=%async_computation.2 | async-start | bytes 1048576 | tf_op jit(solution)/shard_map/all_to_all | solution.py:63
  281.3 12.3 %all-to-all-start.2 = ((f32[8,1,256]{2,1,0:T(1,128)}), f32[8,1,256]{2,1,0:T(1,128)S(1)}, u32[]{:S(2)}, u32[]{:S(2)}) async-start(f32[8,1,256]{2,1,0:T(1,128)} %broadcast_in_dim.8), calls=%async_computation.3 | async-start | bytes 16384 | tf_op jit(solution)/shard_map/all_to_all | solution.py:11
Sparse Core Ops, SparseCore 0:
  96.9 59.9 all-gather.1
  170.4 60.1 reduce-scatter.1
where the time goes:
time: 302 us; the launch traced here: 301 us
  waiting for transfers between devices  161 us (53%)
  blocking collectives  77.5 us (26%)
  starting transfers between devices  18.4 us (6%)
  between operations  13.6 us (5%)
  matrix products  13.4 us (4%)
  local copies, waits for them, and re-layouts  11.1 us (4%)
  other arithmetic  6.13 us (2%)
    all_to_all x1, blocking collectives, on_device(): lax.all_to_all(outgoing, 'ep', split_axis=0, concat_axis=0, tiled=True)  77.5 us
    reduce_scatter x1, waiting for transfers between devices, on_device(): lax.psum_scatter(lax.dot_general(w_down, act, (((0,), (1,)), ((), ())), p...  60.4 us
    all_gather x1, waiting for transfers between devices, on_device(): piece = lax.all_gather(arrived, 'tp', axis=1, tiled=True)  60 us
    all_to_all x1, waiting for transfers between devices, on_device(): lax.all_to_all(summed, 'ep', split_axis=1, concat_axis=1, tiled=True)  32.9 us
    all_to_all x1, starting transfers between devices, on_device(): lax.all_to_all(summed, 'ep', split_axis=1, concat_axis=1, tiled=True)  13.8 us
    dot_general x1, matrix products, on_device(): lax.dot_general(w_down, act, (((0,), (1,)), ((), ())), preferred_element_...  8.85 us
    all_to_all x1, waiting for transfers between devices, copy_for_each(): return lax.all_to_all(copies, axis, split_axis=0, concat_axis=0, tiled=True)  7.71 us
  transfers between devices with their start and end apart: 4, of which 4 were waited for; matrix products, arithmetic and copies ran while one was open for 0% of the time, Pallas kernels for 0%

commit v1 on v0

v1 whole, which is shorter than its diff:
```python
import functools

import jax
import jax.numpy as jnp
from jax import lax
from jax.experimental import pallas as pl
from jax.experimental.pallas import tpu as pltpu
from jax.sharding import PartitionSpec as P

eps = 1e-05
MESH = pl.DeviceIdType.MESH
F32 = jnp.float32
BF16 = jnp.bfloat16


def source_order(chips):
    offsets = sorted(range(-(chips // 2) + 1, chips // 2 + 1), key=lambda d: (abs(d), d))
    return [d for d in offsets if d % 2 == 0] + [d for d in offsets[::-1] if d % 2 == 1]


def layer(
    n_ep, n_tp, chunks, stride,
    tokens, in_gain, ids, ids_row, route, w_gate_hbm, w_up_hbm, w_down_hbm, out_gain,
    out,
    tok, w_gate, w_up, w_down, outgoing, rows, part_in, part_out, act, total_out, returned, mix_hi, mix_lo,
    sq_send, sq_recv,
    load_sem, disp_send, disp_recv, ag_send, ag_recv, rs_send, rs_recv, ret_send, ret_recv, sq_ssem, sq_rsem,
):
    tok_count, width = tok.shape
    top = ids.shape[1]
    experts = n_ep
    slots = rows.shape[0] // n_tp // n_ep
    feat = width // n_tp
    row_count = n_ep * slots
    per = n_ep // chunks
    size = per * slots
    half = size // 2
    hops = n_tp // 2
    me_t = lax.axis_index("tp")
    me_e = lax.axis_index("ep")
    chip = me_e // 2
    core = lax.rem(me_e, 2)
    chips = n_ep // 2
    right = lax.rem(me_t + 1, n_tp)
    left = lax.rem(me_t + n_tp - 1, n_tp)
    order = [(d, c) for d in source_order(chips) for c in (0, 1)]

    def at_tp(offset):
        return lax.rem(me_t + offset + 2 * n_tp, n_tp)

    def at_ep(offset, other):
        return lax.rem(chip + offset + 2 * chips, chips) * 2 + lax.rem(core + other, 2)

    def block(j, start, count):
        return rows.at[pl.ds(pl.multiple_of(j * row_count + start, slots), count)]

    loads = [pltpu.make_async_copy(tokens, tok, load_sem.at[0])]
    loads.append(pltpu.make_async_copy(w_gate_hbm, w_gate, load_sem.at[1]))
    loads.append(pltpu.make_async_copy(w_up_hbm, w_up, load_sem.at[2]))
    for j in range(n_tp):
        loads.append(
            pltpu.make_async_copy(
                w_down_hbm.at[:, pl.ds(j * feat, feat)], w_down.at[j], load_sem.at[3 + j]
            )
        )
    for load in loads:
        load.start()

    barrier = pltpu.get_barrier_semaphore()
    for j in range(1, n_ep):
        pl.semaphore_signal(
            barrier, inc=1, device_id={"ep": lax.rem(me_e + j, n_ep)}, device_id_type=MESH
        )
    for j in range(1, n_tp):
        pl.semaphore_signal(barrier, inc=1, device_id={"tp": at_tp(j)}, device_id_type=MESH)

    expert = lax.broadcasted_iota(jnp.int32, (experts, tok_count), 0)
    named = ids_row[0:1, :] == expert
    for k in range(1, top):
        named = named | (ids_row[k : k + 1, :] == expert)
    first = lax.broadcasted_iota(jnp.int32, (tok_count, tok_count), 0)
    second = lax.broadcasted_iota(jnp.int32, (tok_count, tok_count), 1)
    earlier = jnp.dot(
        jnp.where(named, 1.0, 0.0).astype(BF16),
        jnp.where(first < second, 1.0, 0.0).astype(BF16),
        preferred_element_type=F32,
    )
    key = jnp.where(named, earlier, -1.0)
    slot_of = lax.broadcasted_iota(jnp.int32, (slots, tok_count), 0).astype(F32)

    loads[0].wait()
    squares = jnp.zeros((tok_count, 128), F32)
    for j in range(width // 128):
        piece = tok[:, j * 128 : (j + 1) * 128].astype(F32)
        squares = squares + piece * piece
    mean = jnp.sum(squares, axis=1, keepdims=True) / width
    mine = pl.ds(pl.multiple_of(me_t * feat, feat), feat)
    normed = (
        tok[:, mine].astype(F32) * lax.rsqrt(mean + eps) * in_gain[:, mine].astype(F32)
    ).astype(BF16)
    group = max(1, 256 // slots)
    for e in range(0, experts, group):
        pick = jnp.concatenate(
            [
                jnp.where(key[i : i + 1, :] == slot_of, 1.0, 0.0).astype(BF16)
                for i in range(e, min(experts, e + group))
            ],
            axis=0,
        )
        outgoing[e * slots : e * slots + pick.shape[0], :] = jnp.dot(
            pick, normed, preferred_element_type=F32
        ).astype(BF16)

    pl.semaphore_wait(barrier, n_ep - 1 + n_tp - 1)

    for k in range(1, n_ep):
        offset, other = order[k]
        peer = at_ep(-offset, other)
        pltpu.make_async_remote_copy(
            src_ref=outgoing.at[pl.ds(pl.multiple_of(peer * slots, slots), slots)],
            dst_ref=block(me_t, k * slots, slots),
            send_sem=disp_send,
            recv_sem=disp_recv.at[k // per],
            device_id={"ep": peer},
            device_id_type=MESH,
        ).start()
    rows[pl.ds(pl.multiple_of(me_t * row_count, slots), slots), :] = outgoing[
        pl.ds(pl.multiple_of(me_e * slots, slots), slots), :
    ]

    def forward(c, s, way, j, start, count):
        pltpu.make_async_remote_copy(
            src_ref=block(j, start, count),
            dst_ref=block(j, start, count),
            send_sem=ag_send.at[way],
            recv_sem=ag_recv.at[way, c, s],
            device_id={"tp": right if way == 0 else left},
            device_id_type=MESH,
        ).start()

    def wait_for(ref, sem, send=False):
        copy = pltpu.make_async_remote_copy(
            src_ref=ref, dst_ref=ref, send_sem=sem, recv_sem=sem, device_id={"tp": right}, device_id_type=MESH
        )
        if send:
            copy.wait_send()
        else:
            copy.wait_recv()

    def piece_of(s, way, start):
        if s < hops - 1:
            return start, size
        return (start, half) if way == 0 else (start + half, half)

    def gather_step(c, s):
        start = c * size
        if s == 0:
            skip = slots if c == 0 else 0
            wait_for(block(me_t, start + skip, size - skip), disp_recv.at[c])
        for way in (0, 1):
            step = -1 if way == 0 else 1
            j = at_tp(step * s)
            if s > 0:
                wait_for(block(j, *piece_of(s - 1, way, start)), ag_recv.at[way, c, s - 1])
            if s < hops:
                forward(c, s, way, j, *piece_of(s, way, start))
        if s == hops:
            if c == 0:
                for load in loads[1:]:
                    load.wait()
            x = jnp.concatenate(
                [rows[j * row_count + start : j * row_count + start + size, :] for j in range(n_tp)],
                axis=1,
            )
            gate = jnp.minimum(jnp.dot(x, w_gate[...], preferred_element_type=F32), 7.0)
            up = jnp.clip(jnp.dot(x, w_up[...], preferred_element_type=F32), -7.0, 7.0)
            act[start : start + size, :] = (
                gate * jax.nn.sigmoid(1.702 * gate) * (up + 1.0)
            ).astype(BF16)

    def sum_step(c, s):
        start = c * size
        if s == 0:
            own = jnp.dot(act[start : start + size, :], w_down[at_tp(hops)], preferred_element_type=F32)
            part_out[0, c, 0, 0:half, :] = own[0:half, :].astype(BF16)
            part_out[1, c, 0, half:size, :] = own[half:size, :].astype(BF16)
        elif s < hops:
            own = [
                jnp.dot(
                    act[start : start + size, :],
                    w_down[at_tp(hops - s if way == 0 else s - hops)],
                    preferred_element_type=F32,
                )
                for way in (0, 1)
            ]
            for way in (0, 1):
                if s == 1:
                    lo = 0 if way == 0 else half
                    wait_for(part_in.at[way, c, 0, pl.ds(lo, half)], rs_recv.at[way, c, 0])
                    fresh = slice(half, size) if way == 0 else slice(0, half)
                    part_out[way, c, 1, lo : lo + half, :] = (
                        own[way][lo : lo + half, :] + part_in[way, c, 0, lo : lo + half, :].astype(F32)
                    ).astype(BF16)
                    part_out[way, c, 1, fresh, :] = own[way][fresh, :].astype(BF16)
                else:
                    wait_for(part_in.at[way, c, s - 1], rs_recv.at[way, c, s - 1])
                    part_out[way, c, s] = (own[way] + part_in[way, c, s - 1].astype(F32)).astype(BF16)
                send_part(c, s, way)
            return
        if s == 0:
            for way in (0, 1):
                send_part(c, 0, way)
            return
        own = jnp.dot(act[start : start + size, :], w_down[me_t], preferred_element_type=F32)
        for way in (0, 1):
            if hops == 1:
                lo = 0 if way == 0 else half
                wait_for(part_in.at[way, c, 0, pl.ds(lo, half)], rs_recv.at[way, c, 0])
            else:
                wait_for(part_in.at[way, c, s - 1], rs_recv.at[way, c, s - 1])
        if hops == 1:
            arrived = jnp.concatenate(
                [part_in[0, c, 0, 0:half, :], part_in[1, c, 0, half:size, :]], axis=0
            ).astype(F32)
        else:
            arrived = part_in[0, c, s - 1].astype(F32) + part_in[1, c, s - 1].astype(F32)
        total_out[start : start + size, :] = (own + arrived).astype(BF16)
        for k in range(c * per, (c + 1) * per):
            offset, other = order[k]
            home = pl.ds(pl.multiple_of(me_e * slots, slots), slots)
            if k == 0:
                returned[home, :] = total_out[0:slots, :]
                continue
            pltpu.make_async_remote_copy(
                src_ref=total_out.at[pl.ds(k * slots, slots)],
                dst_ref=returned.at[home],
                send_sem=ret_send,
                recv_sem=ret_recv,
                device_id={"ep": at_ep(offset, other)},
                device_id_type=MESH,
            ).start()

    def send_part(c, s, way):
        if s == 0:
            piece = pl.ds(0 if way == 0 else half, half)
            src, dst = part_out.at[way, c, 0, piece], part_in.at[way, c, 0, piece]
        else:
            src, dst = part_out.at[way, c, s], part_in.at[way, c, s]
        pltpu.make_async_remote_copy(
            src_ref=src,
            dst_ref=dst,
            send_sem=rs_send.at[way],
            recv_sem=rs_recv.at[way, c, s],
            device_id={"tp": right if way == 0 else left},
            device_id_type=MESH,
        ).start()

    def prepare_mix():
        lane = lax.broadcasted_iota(jnp.int32, (tok_count, experts), 1)
        hits = [ids[:, k : k + 1] == lane for k in range(top)]
        marks = sum(jnp.where(h, 1.0, 0.0) for h in hits).astype(BF16)
        before = jnp.dot(
            jnp.where(second < first, 1.0, 0.0).astype(BF16), marks, preferred_element_type=F32
        )
        dest = [
            ids[:, k : k + 1].astype(F32) * slots
            + jnp.sum(jnp.where(hits[k], before, 0.0), axis=1, keepdims=True)
            for k in range(top)
        ]
        weight = [route[:, k : k + 1] for k in range(top)]
        weight_hi = [w.astype(BF16).astype(F32) for w in weight]
        weight_lo = [w - h for w, h in zip(weight, weight_hi)]
        wide = min(256, row_count)
        for r in range(0, row_count, wide):
            place = (lax.broadcasted_iota(jnp.int32, (tok_count, wide), 1) + r).astype(F32)
            for ref, values in ((mix_hi, weight_hi), (mix_lo, weight_lo)):
                mixed = jnp.zeros((tok_count, wide), F32)
                for k in range(top):
                    mixed = jnp.where(place == dest[k], values[k], mixed)
                ref[:, r : r + wide] = mixed.astype(BF16)

    for tick in range(stride * (chunks - 1) + 2 * hops + 1):
        for c in range(chunks):
            s = tick - stride * c - hops
            if 0 < s <= hops:
                sum_step(c, s)
        for c in range(chunks):
            s = tick - stride * c
            if 0 <= s <= hops:
                gather_step(c, s)
                if s == hops:
                    sum_step(c, 0)
        if tick == 0:
            prepare_mix()

    wait_for(returned.at[pl.ds(0, row_count - slots)], ret_recv)
    combined = jnp.dot(mix_hi[...], returned[...], preferred_element_type=F32) + jnp.dot(
        mix_lo[...], returned[...], preferred_element_type=F32
    )
    own_sq = jnp.broadcast_to(
        jnp.sum(combined * combined, axis=1, keepdims=True), (tok_count, 128)
    ).T[0:8, :]
    sq_send[...] = own_sq
    for j in range(1, n_tp):
        pltpu.make_async_remote_copy(
            src_ref=sq_send,
            dst_ref=sq_recv.at[me_t],
            send_sem=sq_ssem,
            recv_sem=sq_rsem,
            device_id={"tp": at_tp(j)},
            device_id_type=MESH,
        ).start()
    sq_recv[me_t] = own_sq
    wait_for(sq_recv.at[pl.ds(0, n_tp - 1)], sq_rsem)
    sum_sq = sq_recv[0]
    for j in range(1, n_tp):
        sum_sq = sum_sq + sq_recv[j]
    scale = jnp.broadcast_to(lax.rsqrt(sum_sq[0:1, :] / width + eps), (128, tok_count)).T
    out[...] = (
        combined * jnp.concatenate([scale] * (feat // 128), axis=1) * out_gain[...].astype(F32)
    ).astype(BF16)

    wait_for(outgoing.at[pl.ds(0, row_count - slots)], disp_send, True)
    wait_for(total_out.at[pl.ds(0, row_count - slots)], ret_send, True)
    for way in (0, 1):
        sent = (hops - 1) * row_count + row_count // 2
        wait_for(rows.at[pl.ds(0, sent)], ag_send.at[way], True)
        wait_for(rows.at[pl.ds(0, sent)], rs_send.at[way], True)
    wait_for(sq_recv.at[pl.ds(0, n_tp - 1)], sq_ssem, True)


def on_device(
    tokens, in_gain, expert_ids, route_weights, gate_weight, up_weight, down_weight, out_gain
):
    n_ep = lax.axis_size("ep")
    n_tp = lax.axis_size("tp")
    tok_count, width = tokens.shape
    top = expert_ids.shape[1]
    slots = 2 * tok_count * top // n_ep
    feat = width // n_tp
    hidden = gate_weight.shape[2]
    row_count = n_ep * slots
    chunks = max(2, n_ep // 4)
    size = row_count // chunks
    hops = n_tp // 2
    hbm = pl.BlockSpec(memory_space=pl.ANY)
    vmem = pl.BlockSpec(memory_space=pltpu.VMEM)
    dma = pltpu.SemaphoreType.DMA
    return pl.pallas_call(
        functools.partial(layer, n_ep, n_tp, chunks, 2),
        out_shape=jax.ShapeDtypeStruct((tok_count, feat), BF16),
        in_specs=[hbm, vmem, vmem, vmem, vmem, hbm, hbm, hbm, vmem],
        out_specs=vmem,
        scratch_shapes=[
            pltpu.VMEM((tok_count, width), BF16),
            pltpu.VMEM((width, hidden), BF16),
            pltpu.VMEM((width, hidden), BF16),
            pltpu.VMEM((n_tp, hidden, feat), BF16),
            pltpu.VMEM((row_count, feat), BF16),
            pltpu.VMEM((n_tp * row_count, feat), BF16),
            pltpu.VMEM((2, chunks, hops, size, feat), BF16),
            pltpu.VMEM((2, chunks, hops, size, feat), BF16),
            pltpu.VMEM((row_count, hidden), BF16),
            pltpu.VMEM((row_count, feat), BF16),
            pltpu.VMEM((row_count, feat), BF16),
            pltpu.VMEM((tok_count, row_count), BF16),
            pltpu.VMEM((tok_count, row_count), BF16),
            pltpu.VMEM((8, tok_count), F32),
            pltpu.VMEM((n_tp, 8, tok_count), F32),
            dma((3 + n_tp,)),
            dma,
            dma((chunks,)),
            dma((2,)),
            dma((2, chunks, hops)),
            dma((2,)),
            dma((2, chunks, hops)),
            dma,
            dma,
            dma,
            dma,
        ],
        compiler_params=pltpu.CompilerParams(collective_id=0, has_side_effects=True),
        name="layer",
    )(
        tokens,
        in_gain.reshape(1, width),
        expert_ids,
        expert_ids.T,
        route_weights,
        gate_weight[0],
        up_weight[0],
        down_weight[0],
        out_gain.reshape(1, feat),
    )


def solution(mesh):
    placed = (
        P(("grp", "ep"), None),
        P(),
        P(("grp", "ep"), None),
        P(("grp", "ep"), None),
        P("ep", None, "tp"),
        P("ep", None, "tp"),
        P("ep", "tp", None),
        P("tp"),
    )
    return jax.shard_map(
        on_device, mesh=mesh, in_specs=placed, out_specs=P(("grp", "ep"), "tp"), check_vma=False
    )
```

time: 302 us -> 174 us (0.58)
  Pallas kernels: 0 us -> 167 us
  waiting for transfers between devices: 161 us -> 0 us
  blocking collectives: 77.5 us -> 0 us
  starting transfers between devices: 18.4 us -> 0 us
  between operations: 13.6 us -> 0.02 us
  matrix products: 13.4 us -> 0 us
  other arithmetic: 6.13 us -> 0 us
  local copies, waits for them, and re-layouts: 11.1 us -> 5.11 us
    pallas_call x0 -> x1, Pallas kernels: none -> 167 us  [on_device(): pl.pallas_call(functools.partial(layer, n_ep, n_tp, chunks, 2), out_shape...]
    all_to_all x1 -> x0, blocking collectives: 77.5 us -> none  [on_device(): lax.all_to_all(outgoing, 'ep', split_axis=0, concat_axis=0, tiled=True)]
    reduce_scatter x1 -> x0, waiting for transfers between devices: 60.4 us -> none  [on_device(): lax.psum_scatter(lax.dot_general(w_down, act, (((0,), (1,)), ((), ())), p...]
    all_gather x1 -> x0, waiting for transfers between devices: 60 us -> none  [on_device(): piece = lax.all_gather(arrived, 'tp', axis=1, tiled=True)]
    all_to_all x2 -> x0, waiting for transfers between devices: 40.7 us -> none  [the longest x1 32.9 us: on_device(): lax.all_to_all(summed, 'ep', split_axis=1, concat_axis=1, tiled=True)]
    all_to_all x2 -> x0, starting transfers between devices: 18.4 us -> none  [the longest x1 13.8 us: on_device(): lax.all_to_all(summed, 'ep', split_axis=1, concat_axis=1, tiled=True)]
    dot_general x2 -> x0, matrix products: 13.4 us -> none  [the longest x1 8.85 us: on_device(): lax.dot_general(w_down, act, (((0,), (1,)), ((), ())), preferred_element_...]
    gather x2 -> x0, local copies, waits for them, and re-layouts: 5.89 us -> none  [the longest x1 3.94 us: on_device(): outgoing = extended[slot_token].reshape(experts, capacity, source.shape[1])]
  transfers between devices with their start and end apart: 4 -> 0, of which waited for: 4 -> 0; matrix products, arithmetic and copies ran while one was open for 0% -> 0% of each run, Pallas kernels for 0% -> 0%
where the time goes in v1:
time: 174 us; the launch traced here: 172 us
  Pallas kernels  167 us (96%)
  local copies, waits for them, and re-layouts  5.11 us (3%)
    pallas_call x1, Pallas kernels, on_device(): pl.pallas_call(functools.partial(layer, n_ep, n_tp, chunks, 2), out_shape...  167 us
    unnamed x11, local copies, waits for them, and re-layouts  3.92 us

profile of v1, /device:TPU:80, one launch (start us, length us, event | category | flops | bytes accessed | tf_op | source)
XLA Modules:
  0.0 172.2 jit_solution(9098882231324770632)
XLA Ops:
  0.0 0.0 copy-start.1
  0.0 0.0 copy-start.3
  0.0 0.7 copy-done.3
  0.7 0.6 reshape.7.out_gain
  1.3 0.0 copy-done.1
  1.3 0.0 copy-start.2
  1.3 0.6 reshape.6.in_gain
  1.9 0.1 copy-done.2
  2.0 0.0 copy-start
  2.0 0.8 copy.10.route
  2.7 0.0 copy-done
  2.7 0.8 copy.9.ids
  3.5 167.1 %layer.1 = bf16[256,256]{1,0:T(8,128)(2,1)} custom-call(bf16[256,2048]{1,0:T(8,128)(2,1)} %tokens.1, bf16[1,2048]{1,0:T(2,128)(2,1)} %reshape.6.in_gain, s32[256,2]{1,0:T(8,128)} %copy.9.ids, s32[2,256]{1,0:T(2,128)} %bitcast.7, f32[256,2]{1,0:T(8,128)} %copy.10.route, bf16[2048,256]{1,0:T(8,128)(2,1)} %bitcast.4, bf16[2048,256]{1,0:T(8,128)(2,1)} %bitcast.5, ...), custom_call_target="tpu_custom_call" | custom-call | tf_op jit(solution)/shard_map/layer/pallas_call | solution.py:349
  170.7 1.6 copy.12
Async XLA Ops:
  0.0 1.3 copy-start.1
  0.0 0.7 copy-start.3
  1.3 0.7 copy-start.2
  2.0 0.8 copy-start

commit v2 on v1

--- a/solution.py
+++ b/solution.py
@@ -13,21 +13,25 @@
 BF16 = jnp.bfloat16
 
 
-def source_order(chips):
-    offsets = sorted(range(-(chips // 2) + 1, chips // 2 + 1), key=lambda d: (abs(d), d))
-    return [d for d in offsets if d % 2 == 0] + [d for d in offsets[::-1] if d % 2 == 1]
+def notice_plan(n_ep, hops):
+    plan, given, tick = {}, 1, 0
+    while given < n_ep:
+        pace = 2 if tick == 0 else (n_ep + 8) // 10 if tick <= hops else (n_ep + 2) // 5
+        plan[tick] = list(range(given, min(n_ep, given + pace)))
+        given, tick = given + pace, tick + 1
+    return plan
 
 
 def layer(
     n_ep, n_tp, chunks, stride,
-    tokens, in_gain, ids, ids_row, route, w_gate_hbm, w_up_hbm, w_down_hbm, out_gain,
+    tokens, in_gain, ids_row, route_row, w_gate_hbm, w_up_hbm, w_down_hbm, out_gain,
     out,
     tok, w_gate, w_up, w_down, outgoing, rows, part_in, part_out, act, total_out, returned, mix_hi, mix_lo,
     sq_send, sq_recv,
-    load_sem, disp_send, disp_recv, ag_send, ag_recv, rs_send, rs_recv, ret_send, ret_recv, sq_ssem, sq_rsem,
+    load_sem, up_sem, disp_send, disp_recv, ag_send, ag_recv, rs_send, rs_recv, ret_send, ret_recv, sq_ssem, sq_rsem,
 ):
     tok_count, width = tok.shape
-    top = ids.shape[1]
+    top = ids_row.shape[0]
     experts = n_ep
     slots = rows.shape[0] // n_tp // n_ep
     feat = width // n_tp
@@ -38,18 +42,24 @@
     hops = n_tp // 2
     me_t = lax.axis_index("tp")
     me_e = lax.axis_index("ep")
-    chip = me_e // 2
-    core = lax.rem(me_e, 2)
-    chips = n_ep // 2
+    link = lax.rem(me_e + n_ep - 1, n_ep)
     right = lax.rem(me_t + 1, n_tp)
     left = lax.rem(me_t + n_tp - 1, n_tp)
-    order = [(d, c) for d in source_order(chips) for c in (0, 1)]
+    def late_place(at):
+        return (chunks - 1 - at * chunks // n_ep) * per + per - 1
+
+    def place_of(source, at):
+        index = lax.rem(source + n_ep - 1, n_ep)
+        held = late_place(at)
+        after = jnp.where(index >= held, index + 1, index)
+        return jnp.where(source == 0, held, after)
+
+    def source_at(place):
+        held = late_place(me_e)
+        return jnp.where(place == held, 0, jnp.where(place > held, place, place + 1))
 
     def at_tp(offset):
         return lax.rem(me_t + offset + 2 * n_tp, n_tp)
-
-    def at_ep(offset, other):
-        return lax.rem(chip + offset + 2 * chips, chips) * 2 + lax.rem(core + other, 2)
 
     def block(j, start, count):
         return rows.at[pl.ds(pl.multiple_of(j * row_count + start, slots), count)]
@@ -67,10 +77,6 @@
         load.start()
 
     barrier = pltpu.get_barrier_semaphore()
-    for j in range(1, n_ep):
-        pl.semaphore_signal(
-            barrier, inc=1, device_id={"ep": lax.rem(me_e + j, n_ep)}, device_id_type=MESH
-        )
     for j in range(1, n_tp):
         pl.semaphore_signal(barrier, inc=1, device_id={"tp": at_tp(j)}, device_id_type=MESH)
 
@@ -111,20 +117,42 @@
             pick, normed, preferred_element_type=F32
         ).astype(BF16)
 
-    pl.semaphore_wait(barrier, n_ep - 1 + n_tp - 1)
-
-    for k in range(1, n_ep):
-        offset, other = order[k]
-        peer = at_ep(-offset, other)
+    pl.semaphore_wait(barrier, n_tp - 1 + jnp.minimum(link, 1))
+
+    @pl.when(link < n_ep - 1)
+    def _():
+        pl.semaphore_signal(
+            barrier, inc=1, device_id={"ep": lax.rem(me_e + 1, n_ep)}, device_id_type=MESH
+        )
+
+    my_place = place_of(me_e, me_e)
+
+    def dispatch(peer):
+        place = place_of(me_e, peer)
         pltpu.make_async_remote_copy(
             src_ref=outgoing.at[pl.ds(pl.multiple_of(peer * slots, slots), slots)],
-            dst_ref=block(me_t, k * slots, slots),
+            dst_ref=block(me_t, place * slots, slots),
             send_sem=disp_send,
-            recv_sem=disp_recv.at[k // per],
+            recv_sem=disp_recv.at[place],
             device_id={"ep": peer},
             device_id_type=MESH,
         ).start()
-    rows[pl.ds(pl.multiple_of(me_t * row_count, slots), slots), :] = outgoing[
+
+    for d in range(n_ep - 1, 0, -1):
+
+        @pl.when(link >= d)
+        def _(d=d):
+            peer = lax.rem(me_e - d + n_ep, n_ep)
+            pl.semaphore_signal(up_sem.at[d], inc=1, device_id={"ep": peer}, device_id_type=MESH)
+            dispatch(peer)
+
+    def notice(d):
+        @pl.when(link + d < n_ep)
+        def _():
+            pl.semaphore_wait(up_sem.at[d], 1)
+            dispatch(lax.rem(me_e + d, n_ep))
+
+    rows[pl.ds(pl.multiple_of(me_t * row_count + my_place * slots, slots), slots), :] = outgoing[
         pl.ds(pl.multiple_of(me_e * slots, slots), slots), :
     ]
 
@@ -155,8 +183,12 @@
     def gather_step(c, s):
         start = c * size
         if s == 0:
-            skip = slots if c == 0 else 0
-            wait_for(block(me_t, start + skip, size - skip), disp_recv.at[c])
+            for place in range(c * per, (c + 1) * per):
+
+                @pl.when(my_place != place)
+                def _(place=place):
+                    wait_for(block(me_t, place * slots, slots), disp_recv.at[place])
+
         for way in (0, 1):
             step = -1 if way == 0 else 1
             j = at_tp(step * s)
@@ -225,20 +257,23 @@
         else:
             arrived = part_in[0, c, s - 1].astype(F32) + part_in[1, c, s - 1].astype(F32)
         total_out[start : start + size, :] = (own + arrived).astype(BF16)
-        for k in range(c * per, (c + 1) * per):
-            offset, other = order[k]
-            home = pl.ds(pl.multiple_of(me_e * slots, slots), slots)
-            if k == 0:
-                returned[home, :] = total_out[0:slots, :]
-                continue
-            pltpu.make_async_remote_copy(
-                src_ref=total_out.at[pl.ds(k * slots, slots)],
-                dst_ref=returned.at[home],
-                send_sem=ret_send,
-                recv_sem=ret_recv,
-                device_id={"ep": at_ep(offset, other)},
-                device_id_type=MESH,
-            ).start()
+        home = pl.ds(pl.multiple_of(me_e * slots, slots), slots)
+        for place in range(c * per, (c + 1) * per):
+
+            @pl.when(my_place == place)
+            def _(place=place):
+                returned[home, :] = total_out[place * slots : (place + 1) * slots, :]
+
+            @pl.when(my_place != place)
+            def _(place=place):
+                pltpu.make_async_remote_copy(
+                    src_ref=total_out.at[pl.ds(place * slots, slots)],
+                    dst_ref=returned.at[home],
+                    send_sem=ret_send,
+                    recv_sem=ret_recv,
+                    device_id={"ep": source_at(place)},
+                    device_id_type=MESH,
+                ).start()
 
     def send_part(c, s, way):
         if s == 0:
@@ -256,18 +291,22 @@
         ).start()
 
     def prepare_mix():
-        lane = lax.broadcasted_iota(jnp.int32, (tok_count, experts), 1)
-        hits = [ids[:, k : k + 1] == lane for k in range(top)]
+        def column(row):
+            return jnp.broadcast_to(row, (128, tok_count)).T[:, 0:1]
+
+        ids = [column(ids_row[k : k + 1, :].astype(F32)) for k in range(top)]
+        lane = lax.broadcasted_iota(jnp.int32, (tok_count, experts), 1).astype(F32)
+        hits = [ids[k] == lane for k in range(top)]
         marks = sum(jnp.where(h, 1.0, 0.0) for h in hits).astype(BF16)
         before = jnp.dot(
             jnp.where(second < first, 1.0, 0.0).astype(BF16), marks, preferred_element_type=F32
         )
         dest = [
-            ids[:, k : k + 1].astype(F32) * slots
+            ids[k] * slots
             + jnp.sum(jnp.where(hits[k], before, 0.0), axis=1, keepdims=True)
             for k in range(top)
         ]
-        weight = [route[:, k : k + 1] for k in range(top)]
+        weight = [column(route_row[k : k + 1, :]) for k in range(top)]
         weight_hi = [w.astype(BF16).astype(F32) for w in weight]
         weight_lo = [w - h for w, h in zip(weight, weight_hi)]
         wide = min(256, row_count)
@@ -279,11 +318,17 @@
                     mixed = jnp.where(place == dest[k], values[k], mixed)
                 ref[:, r : r + wide] = mixed.astype(BF16)
 
+    plan = notice_plan(n_ep, hops)
     for tick in range(stride * (chunks - 1) + 2 * hops + 1):
+        noticed = plan.get(tick, [])
+        for d in noticed[: len(noticed) // 2]:
+            notice(d)
         for c in range(chunks):
             s = tick - stride * c - hops
             if 0 < s <= hops:
                 sum_step(c, s)
+        for d in noticed[len(noticed) // 2 :]:
+            notice(d)
         for c in range(chunks):
             s = tick - stride * c
             if 0 <= s <= hops:
@@ -347,9 +392,9 @@
     vmem = pl.BlockSpec(memory_space=pltpu.VMEM)
     dma = pltpu.SemaphoreType.DMA
     return pl.pallas_call(
-        functools.partial(layer, n_ep, n_tp, chunks, 2),
+        functools.partial(layer, n_ep, n_tp, chunks, 1),
         out_shape=jax.ShapeDtypeStruct((tok_count, feat), BF16),
-        in_specs=[hbm, vmem, vmem, vmem, vmem, hbm, hbm, hbm, vmem],
+        in_specs=[hbm, vmem, vmem, vmem, hbm, hbm, hbm, vmem],
         out_specs=vmem,
         scratch_shapes=[
             pltpu.VMEM((tok_count, width), BF16),
@@ -368,8 +413,9 @@
             pltpu.VMEM((8, tok_count), F32),
             pltpu.VMEM((n_tp, 8, tok_count), F32),
             dma((3 + n_tp,)),
+            pltpu.SemaphoreType.REGULAR((n_ep,)),
             dma,
-            dma((chunks,)),
+            dma((n_ep,)),
             dma((2,)),
             dma((2, chunks, hops)),
             dma((2,)),
@@ -384,9 +430,8 @@
     )(
         tokens,
         in_gain.reshape(1, width),
-        expert_ids,
         expert_ids.T,
-        route_weights,
+        route_weights.T,
         gate_weight[0],
         up_weight[0],
         down_weight[0],

time: 174 us -> 144 us (0.83)
  Pallas kernels: 167 us -> 140 us
    pallas_call x1, Pallas kernels: 167 us -> 140 us  [on_device(): pl.pallas_call(functools.partial(layer, n_ep, n_tp, chunks, 1), out_shape...]
    unnamed x11 -> x5, local copies, waits for them, and re-layouts: 3.92 us -> 2.24 us
where the time goes in v2:
time: 144 us; the launch traced here: 143 us
  Pallas kernels  140 us (97%)
  local copies, waits for them, and re-layouts  3.41 us (2%)
    pallas_call x1, Pallas kernels, on_device(): pl.pallas_call(functools.partial(layer, n_ep, n_tp, chunks, 1), out_shape...  140 us

profile of v2, /device:TPU:80, one launch (start us, length us, event | category | flops | bytes accessed | tf_op | source)
XLA Modules:
  0.0 143.4 jit_solution(7724708405441164519)
XLA Ops:
  0.0 0.0 copy-start
  0.0 0.0 copy-start.1
  0.0 0.7 copy-done.1
  0.7 0.6 reshape.7.out_gain
  1.2 0.0 copy-done
  1.2 0.6 reshape.6.in_gain
  1.8 140.0 %layer.1 = bf16[256,256]{1,0:T(8,128)(2,1)} custom-call(bf16[256,2048]{1,0:T(8,128)(2,1)} %tokens.1, bf16[1,2048]{1,0:T(2,128)(2,1)} %reshape.6.in_gain, s32[2,256]{1,0:T(2,128)} %bitcast.8, f32[2,256]{1,0:T(2,128)} %bitcast.9, bf16[2048,256]{1,0:T(8,128)(2,1)} %bitcast.5, bf16[2048,256]{1,0:T(8,128)(2,1)} %bitcast.6, bf16[256,2048]{1,0:T(8,128)(2,1)} %bitcast.7, ...), custom_call_target="tpu_custom_call" | custom-call | tf_op jit(solution)/shard_map/layer/pallas_call | solution.py:394
  141.9 1.6 %copy.10 = bf16[256,256]{1,0:T(8,128)(2,1)} copy(bf16[256,256]{1,0:T(8,128)(2,1)} %layer.1) | data formatting | bytes 262144
Async XLA Ops:
  0.0 1.2 copy-start
  0.0 0.7 copy-start.1

commit v3 on v2

--- a/solution.py
+++ b/solution.py
@@ -13,12 +13,26 @@
 BF16 = jnp.bfloat16
 
 
-def notice_plan(n_ep, hops):
-    plan, given, tick = {}, 1, 0
-    while given < n_ep:
-        pace = 2 if tick == 0 else (n_ep + 8) // 10 if tick <= hops else (n_ep + 2) // 5
-        plan[tick] = list(range(given, min(n_ep, given + pace)))
-        given, tick = given + pace, tick + 1
+def schedule(n_ep, chunks, begin, hops):
+    last = max(begin) + 2 * hops
+    starts = [0.0]
+    for tick in range(last):
+        busy = sum(0 <= tick - b < 2 * hops for b in begin)
+        starts.append(starts[-1] + max(3.5, 1.25 * busy))
+    steps = []
+    for tick in range(last + 1):
+        now = [("sum", c, tick - begin[c] - hops) for c in range(chunks) if 0 < tick - begin[c] - hops <= hops]
+        now += [("gather", c, tick - begin[c]) for c in range(chunks) if 0 <= tick - begin[c] <= hops]
+        length = starts[tick + 1] - starts[tick] if tick + 1 < len(starts) else 0.0
+        steps += [(starts[tick] + length * i / len(now), step) for i, step in enumerate(now)]
+    plan, given = [], 1
+    for start, step in steps:
+        come = []
+        while given < n_ep and given * 45.0 / n_ep + 1.5 <= start:
+            come.append(given)
+            given += 1
+        plan.append((come, step))
+    plan[-1] = (plan[-1][0] + list(range(given, n_ep)), plan[-1][1])
     return plan
 
 
@@ -26,7 +40,7 @@
     n_ep, n_tp, chunks, stride,
     tokens, in_gain, ids_row, route_row, w_gate_hbm, w_up_hbm, w_down_hbm, out_gain,
     out,
-    tok, w_gate, w_up, w_down, outgoing, rows, part_in, part_out, act, total_out, returned, mix_hi, mix_lo,
+    tok, w_gate, w_up, w_down, outgoing, rows, part_in, part_out, own_part, total_out, returned, mix_hi, mix_lo,
     sq_send, sq_recv,
     load_sem, up_sem, disp_send, disp_recv, ag_send, ag_recv, rs_send, rs_recv, ret_send, ret_recv, sq_ssem, sq_rsem,
 ):
@@ -45,18 +59,23 @@
     link = lax.rem(me_e + n_ep - 1, n_ep)
     right = lax.rem(me_t + 1, n_tp)
     left = lax.rem(me_t + n_tp - 1, n_tp)
-    def late_place(at):
-        return (chunks - 1 - at * chunks // n_ep) * per + per - 1
+    def layout(at):
+        group = lax.rem(at + n_ep - 1, n_ep) // per
+        final = group == chunks - 1
+        held = jnp.where(final, 0, jnp.minimum(chunks - 1, chunks - group)) * per + per - 1
+        return group * per, jnp.where(final, per - 1, per), held
 
     def place_of(source, at):
-        index = lax.rem(source + n_ep - 1, n_ep)
-        held = late_place(at)
-        after = jnp.where(index >= held, index + 1, index)
-        return jnp.where(source == 0, held, after)
+        begin, own, held = layout(at)
+        index = source - 1
+        rank = jnp.where(index < begin, index + own, jnp.where(index < begin + own, index - begin, index))
+        return jnp.where(source == 0, held, jnp.where(rank >= held, rank + 1, rank))
 
     def source_at(place):
-        held = late_place(me_e)
-        return jnp.where(place == held, 0, jnp.where(place > held, place, place + 1))
+        begin, own, held = layout(me_e)
+        rank = jnp.where(place > held, place - 1, place)
+        other = jnp.where(rank - own < begin, rank - own, rank)
+        return jnp.where(place == held, 0, jnp.where(rank < own, begin + rank, other) + 1)
 
     def at_tp(offset):
         return lax.rem(me_t + offset + 2 * n_tp, n_tp)
@@ -67,12 +86,7 @@
     loads = [pltpu.make_async_copy(tokens, tok, load_sem.at[0])]
     loads.append(pltpu.make_async_copy(w_gate_hbm, w_gate, load_sem.at[1]))
     loads.append(pltpu.make_async_copy(w_up_hbm, w_up, load_sem.at[2]))
-    for j in range(n_tp):
-        loads.append(
-            pltpu.make_async_copy(
-                w_down_hbm.at[:, pl.ds(j * feat, feat)], w_down.at[j], load_sem.at[3 + j]
-            )
-        )
+    loads.append(pltpu.make_async_copy(w_down_hbm, w_down, load_sem.at[3]))
     for load in loads:
         load.start()
 
@@ -102,7 +116,7 @@
     mean = jnp.sum(squares, axis=1, keepdims=True) / width
     mine = pl.ds(pl.multiple_of(me_t * feat, feat), feat)
     normed = (
-        tok[:, mine].astype(F32) * lax.rsqrt(mean + eps) * in_gain[:, mine].astype(F32)
+        tok[:, mine].astype(F32) * lax.rsqrt(mean + eps) * in_gain[mine].astype(F32).reshape(1, feat)
     ).astype(BF16)
     group = max(1, 256 // slots)
     for e in range(0, experts, group):
@@ -138,16 +152,24 @@
             device_id_type=MESH,
         ).start()
 
-    for d in range(n_ep - 1, 0, -1):
+    my_group = link // per
+    for d in range(1, n_ep):
 
         @pl.when(link >= d)
         def _(d=d):
-            peer = lax.rem(me_e - d + n_ep, n_ep)
-            pl.semaphore_signal(up_sem.at[d], inc=1, device_id={"ep": peer}, device_id_type=MESH)
-            dispatch(peer)
-
-    def notice(d):
-        @pl.when(link + d < n_ep)
+            pl.semaphore_signal(
+                up_sem.at[d], inc=1, device_id={"ep": lax.rem(me_e - d + n_ep, n_ep)}, device_id_type=MESH
+            )
+
+    def send_back(d, due):
+        @pl.when(due)
+        def _():
+            dispatch(lax.rem(me_e - d + n_ep, n_ep))
+
+    for d in range(1, per):
+        send_back(d, lax.rem(link, per) >= d)
+    def notice(d, due):
+        @pl.when(due)
         def _():
             pl.semaphore_wait(up_sem.at[d], 1)
             dispatch(lax.rem(me_e + d, n_ep))
@@ -206,23 +228,20 @@
             )
             gate = jnp.minimum(jnp.dot(x, w_gate[...], preferred_element_type=F32), 7.0)
             up = jnp.clip(jnp.dot(x, w_up[...], preferred_element_type=F32), -7.0, 7.0)
-            act[start : start + size, :] = (
-                gate * jax.nn.sigmoid(1.702 * gate) * (up + 1.0)
-            ).astype(BF16)
+            act = (gate * jax.nn.sigmoid(1.702 * gate) * (up + 1.0)).astype(BF16)
+            product = jnp.dot(act, w_down[...], preferred_element_type=F32)
+            for j in range(n_tp):
+                own_part[j, start : start + size, :] = product[:, j * feat : (j + 1) * feat]
 
     def sum_step(c, s):
         start = c * size
         if s == 0:
-            own = jnp.dot(act[start : start + size, :], w_down[at_tp(hops)], preferred_element_type=F32)
+            own = own_part[at_tp(hops), start : start + size, :]
             part_out[0, c, 0, 0:half, :] = own[0:half, :].astype(BF16)
             part_out[1, c, 0, half:size, :] = own[half:size, :].astype(BF16)
         elif s < hops:
             own = [
-                jnp.dot(
-                    act[start : start + size, :],
-                    w_down[at_tp(hops - s if way == 0 else s - hops)],
-                    preferred_element_type=F32,
-                )
+                own_part[at_tp(hops - s if way == 0 else s - hops), start : start + size, :]
                 for way in (0, 1)
             ]
             for way in (0, 1):
@@ -243,7 +262,7 @@
             for way in (0, 1):
                 send_part(c, 0, way)
             return
-        own = jnp.dot(act[start : start + size, :], w_down[me_t], preferred_element_type=F32)
+        own = own_part[me_t, start : start + size, :]
         for way in (0, 1):
             if hops == 1:
                 lo = 0 if way == 0 else half
@@ -318,25 +337,42 @@
                     mixed = jnp.where(place == dest[k], values[k], mixed)
                 ref[:, r : r + wide] = mixed.astype(BF16)
 
-    plan = notice_plan(n_ep, hops)
-    for tick in range(stride * (chunks - 1) + 2 * hops + 1):
-        noticed = plan.get(tick, [])
-        for d in noticed[: len(noticed) // 2]:
-            notice(d)
-        for c in range(chunks):
-            s = tick - stride * c - hops
-            if 0 < s <= hops:
+    for d in range(1, per):
+        notice(d, lax.rem(link, per) + d < per)
+    for d in range(n_ep - 1, 0, -1):
+        send_back(d, (link >= d) & (lax.rem(link, per) < d))
+    def run(begin):
+        looked, reached, passed = set(), 0, 0
+        for number, (come, (kind, c, s)) in enumerate(schedule(n_ep, chunks, begin, hops)):
+            seen = jnp.where(reached > my_group, passed, my_group)
+            for d in come:
+                looked.add(d)
+                notice(d, (link + d < n_ep) & ((link + d) // per > seen))
+            if kind == "gather" and s == 0 and c > 0:
+                until = min(chunks - 1, c + (1 if c < 3 else 2))
+                for d in range(1, min(n_ep, per * (until + 1))):
+                    if d not in looked:
+                        group = (link + d) // per
+                        notice(d, (link + d < n_ep) & (c > my_group) & (group <= until) & (group > seen))
+                reached, passed = c, until
+            if kind == "sum":
                 sum_step(c, s)
-        for d in noticed[len(noticed) // 2 :]:
-            notice(d)
-        for c in range(chunks):
-            s = tick - stride * c
-            if 0 <= s <= hops:
+            else:
                 gather_step(c, s)
                 if s == hops:
                     sum_step(c, 0)
-        if tick == 0:
-            prepare_mix()
+            if number == 0:
+                prepare_mix()
+
+    early = my_group < chunks // 2
+
+    @pl.when(early)
+    def _():
+        run([0, 2, 4, 6, 8, 9, 10, 11])
+
+    @pl.when(jnp.logical_not(early))
+    def _():
+        run(list(range(chunks)))
 
     wait_for(returned.at[pl.ds(0, row_count - slots)], ret_recv)
     combined = jnp.dot(mix_hi[...], returned[...], preferred_element_type=F32) + jnp.dot(
@@ -362,7 +398,7 @@
         sum_sq = sum_sq + sq_recv[j]
     scale = jnp.broadcast_to(lax.rsqrt(sum_sq[0:1, :] / width + eps), (128, tok_count)).T
     out[...] = (
-        combined * jnp.concatenate([scale] * (feat // 128), axis=1) * out_gain[...].astype(F32)
+        combined * jnp.concatenate([scale] * (feat // 128), axis=1) * out_gain[...].astype(F32).reshape(1, feat)
     ).astype(BF16)
 
     wait_for(outgoing.at[pl.ds(0, row_count - slots)], disp_send, True)
@@ -400,19 +436,19 @@
             pltpu.VMEM((tok_count, width), BF16),
             pltpu.VMEM((width, hidden), BF16),
             pltpu.VMEM((width, hidden), BF16),
-            pltpu.VMEM((n_tp, hidden, feat), BF16),
+            pltpu.VMEM((hidden, width), BF16),
             pltpu.VMEM((row_count, feat), BF16),
             pltpu.VMEM((n_tp * row_count, feat), BF16),
             pltpu.VMEM((2, chunks, hops, size, feat), BF16),
             pltpu.VMEM((2, chunks, hops, size, feat), BF16),
-            pltpu.VMEM((row_count, hidden), BF16),
+            pltpu.VMEM((n_tp, row_count, feat), F32),
             pltpu.VMEM((row_count, feat), BF16),
             pltpu.VMEM((row_count, feat), BF16),
             pltpu.VMEM((tok_count, row_count), BF16),
             pltpu.VMEM((tok_count, row_count), BF16),
             pltpu.VMEM((8, tok_count), F32),
             pltpu.VMEM((n_tp, 8, tok_count), F32),
-            dma((3 + n_tp,)),
+            dma((4,)),
             pltpu.SemaphoreType.REGULAR((n_ep,)),
             dma,
             dma((n_ep,)),
@@ -429,13 +465,13 @@
         name="layer",
     )(
         tokens,
-        in_gain.reshape(1, width),
+        in_gain,
         expert_ids.T,
         route_weights.T,
         gate_weight[0],
         up_weight[0],
         down_weight[0],
-        out_gain.reshape(1, feat),
+        out_gain,
     )
 
 

time: 144 us -> 142 us (0.986)
  local copies, waits for them, and re-layouts: 3.41 us -> 1.57 us
where the time goes in v3:
time: 142 us
  Pallas kernels  140 us (99%)
  local copies, waits for them, and re-layouts  1.57 us (1%)
    pallas_call x1, Pallas kernels, on_device(): pl.pallas_call(functools.partial(layer, n_ep, n_tp, chunks, 1), out_shape...  140 us

profile of v3, /device:TPU:80, one launch (start us, length us, event | category | flops | bytes accessed | tf_op | source)
XLA Modules:
  0.0 141.5 jit_solution(10950944161143903163)
XLA Ops:
  0.0 139.9 %layer.1 = bf16[256,256]{1,0:T(8,128)(2,1)} custom-call(bf16[256,2048]{1,0:T(8,128)(2,1)} %tokens.1, bf16[2048]{0:T(1024)(128)(2,1)} %in_gain.1, s32[2,256]{1,0:T(2,128)} %bitcast.8, f32[2,256]{1,0:T(2,128)} %bitcast.9, bf16[2048,256]{1,0:T(8,128)(2,1)} %bitcast.5, bf16[2048,256]{1,0:T(8,128)(2,1)} %bitcast.6, bf16[256,2048]{1,0:T(8,128)(2,1)} %bitcast.7, ...), custom_call_target="tpu_custom_call" | custom-call | tf_op jit(solution)/shard_map/layer/pallas_call | solution.py:430
  139.9 1.6 %copy.10 = bf16[256,256]{1,0:T(8,128)(2,1)} copy(bf16[256,256]{1,0:T(8,128)(2,1)} %layer.1) | data formatting | bytes 262144

commit v4 on v3

--- a/solution.py
+++ b/solution.py
@@ -429,7 +429,7 @@
     dma = pltpu.SemaphoreType.DMA
     return pl.pallas_call(
         functools.partial(layer, n_ep, n_tp, chunks, 1),
-        out_shape=jax.ShapeDtypeStruct((tok_count, feat), BF16),
+        out_shape=pltpu.VMEM((tok_count, feat), BF16),
         in_specs=[hbm, vmem, vmem, vmem, hbm, hbm, hbm, vmem],
         out_specs=vmem,
         scratch_shapes=[

time: 142 us -> 140 us (0.986)
  no operation moved by 1% of the time
where the time goes in v4:
time: 140 us
  Pallas kernels  139 us (99%)
    pallas_call x1, Pallas kernels, on_device(): pl.pallas_call(functools.partial(layer, n_ep, n_tp, chunks, 1), out_shape...  139 us

profile of v4, /device:TPU:80, one launch (start us, length us, event | category | flops | bytes accessed | tf_op | source)
XLA Modules:
  0.0 140.0 jit_solution(17778239255118452231)
XLA Ops:
  0.0 139.3 %layer.1 = bf16[256,256]{1,0:T(8,128)(2,1)S(1)} custom-call(bf16[256,2048]{1,0:T(8,128)(2,1)} %tokens.1, bf16[2048]{0:T(1024)(128)(2,1)} %in_gain.1, s32[2,256]{1,0:T(2,128)} %bitcast.8, f32[2,256]{1,0:T(2,128)} %bitcast.9, bf16[2048,256]{1,0:T(8,128)(2,1)} %bitcast.5, bf16[2048,256]{1,0:T(8,128)(2,1)} %bitcast.6, bf16[256,2048]{1,0:T(8,128)(2,1)} %bitcast.7, ...), custom_call_target="tpu_custom_call" | custom-call | tf_op jit(solution)/shard_map/layer/pallas_call | solution.py:430
  139.3 0.7 copy.10
